TPU v7x, 32 devices: a whole 2x2x4 slice. The times are simulated.
32 devices in a mesh: sp: 8 (over z, y), dp: 4 (over x, core).
Axes of the slice: x: 2, y: 2, z: 4, core: 2. Of those that a mesh axis runs over, the one named last changes fastest.
Arguments:
- query: bfloat16 [4, 1536, 3072], P('dp', 'sp'), may hold values from -18 to 18
- latent: bfloat16 [4, 1536, 1024], P('dp', 'sp'), may hold values from -6 to 6
- rope_key: bfloat16 [4, 1536, 32], P('dp', 'sp'), may hold values from -5 to 5
- latent_norm_gain: float32 [1024], replicated, may hold values from 0.1 to 1.9
- key_up_matrix: bfloat16 [2048, 1024], P('dp'), may hold values from -0.1875 to 0.1875
- value_up_matrix: bfloat16 [2048, 1024], P('dp'), may hold values from -0.1875 to 0.1875
- out_grad: bfloat16 [4, 1536, 2048], P('dp', 'sp'), may hold values from -6 to 6
Outputs:
- query_grad: bfloat16 [4, 1536, 3072], P('dp', 'sp')
- latent_grad: float32 [4, 1536, 1024], P('dp', 'sp')
- rope_key_grad: float32 [4, 1536, 32], P('dp', 'sp')
- key_weight_grad: float32 [2048, 1024], P('dp')
- value_weight_grad: float32 [2048, 1024], P('dp')
- gain_grad: float32 [1024], replicated
All inputs are finite; a program needn't handle non-finite values.
Results may differ from a plain program's by a relative error of at most 0.011.
Values may be sent and summed in bfloat16 or wider, within the bound.
A program may use at most 256 MiB of HBM per device.

v0:
```python
import jax
import jax.numpy as jnp
from jax import lax
from jax.sharding import PartitionSpec as P

ATTENTION_HEADS = 32
PLAIN_HEAD_WIDTH = 64
ROPE = 32
VALUE_HEAD_WIDTH = 64
SPAN = 64
eps = 1e-06
rope_base = 10000.0


def rotate(values, cosine, sine):
    half = values.shape[-1] // 2
    first = values[..., :half]
    second = values[..., half:]
    return jnp.concatenate(
        [first * cosine - second * sine, second * cosine + first * sine], axis=-1
    )


def angles(length, width):
    inverse = 1.0 / rope_base ** (jnp.arange(0, width, 2, dtype=jnp.float32) / width)
    turned = jnp.arange(length, dtype=jnp.float32)[:, None] * inverse[None, :]
    return (jnp.cos(turned), jnp.sin(turned))


def attend_backward(arrived, rope_full):
    f32 = jnp.float32
    bf16 = jnp.bfloat16
    length = arrived.shape[0]
    local_heads = arrived.shape[1]
    width = PLAIN_HEAD_WIDTH + ROPE
    scale = width ** (-0.5)
    block = 512
    cosine, sine = angles(length, ROPE)
    neg = jnp.finfo(f32).min
    q_nope = arrived[:, :, :PLAIN_HEAD_WIDTH]
    q_rope = rotate(
        arrived[:, :, PLAIN_HEAD_WIDTH:width].astype(f32), cosine[:, None, :], sine[:, None, :]
    ).astype(bf16)
    key_nope = arrived[:, :, width : width + PLAIN_HEAD_WIDTH]
    values = arrived[:, :, width + PLAIN_HEAD_WIDTH : width + PLAIN_HEAD_WIDTH + VALUE_HEAD_WIDTH]
    d_out = arrived[:, :, width + PLAIN_HEAD_WIDTH + VALUE_HEAD_WIDTH :]
    k_rope = rotate(rope_full.astype(f32), cosine, sine).astype(bf16)
    dk_nope = jnp.zeros((length, local_heads, PLAIN_HEAD_WIDTH), f32)
    dk_rope = jnp.zeros((length, ROPE), f32)
    d_vals = jnp.zeros((length, local_heads, VALUE_HEAD_WIDTH), f32)
    dq_parts = []
    for begin in range(0, length, block):
        end = begin + block
        qn = q_nope[begin:end]
        qr = q_rope[begin:end]
        go = d_out[begin:end]
        scores = jnp.einsum("qhd,khd->hqk", qn, key_nope[:end], preferred_element_type=f32)
        scores = (
            scores + jnp.einsum("qhd,kd->hqk", qr, k_rope[:end], preferred_element_type=f32)
        ) * scale
        q_seg = jnp.arange(begin, end) // SPAN
        k_seg = jnp.arange(end) // SPAN
        allowed = k_seg[None, :] <= q_seg[:, None]
        scores = jnp.where(allowed[None], scores, neg)
        probs = jax.nn.softmax(scores, axis=-1)
        d_probs = jnp.einsum("qhd,khd->hqk", go, values[:end], preferred_element_type=f32)
        d_scores = probs * (d_probs - jnp.sum(probs * d_probs, axis=-1, keepdims=True))
        ds_b = d_scores.astype(bf16)
        p_b = probs.astype(bf16)
        dq_n = jnp.einsum("hqk,khd->qhd", ds_b, key_nope[:end], preferred_element_type=f32) * scale
        dq_r = jnp.einsum("hqk,kd->qhd", ds_b, k_rope[:end], preferred_element_type=f32) * scale
        dq_r = rotate(dq_r, cosine[begin:end, None, :], -sine[begin:end, None, :])
        dq_parts.append(jnp.concatenate([dq_n, dq_r], axis=-1).astype(bf16))
        dk_nope = dk_nope.at[:end].add(
            jnp.einsum("hqk,qhd->khd", ds_b, qn, preferred_element_type=f32) * scale
        )
        dk_rope = dk_rope.at[:end].add(
            jnp.einsum("hqk,qhd->kd", ds_b, qr, preferred_element_type=f32) * scale
        )
        d_vals = d_vals.at[:end].add(
            jnp.einsum("hqk,qhd->khd", p_b, go, preferred_element_type=f32)
        )
    query_part = jnp.concatenate(dq_parts, axis=0)
    grads = jnp.concatenate([query_part, dk_nope.astype(bf16), d_vals.astype(bf16)], axis=-1)
    return (grads, rotate(dk_rope, cosine, -sine))


def local(query, latent, rope_key, latent_norm_gain, key_up_matrix, value_up_matrix, out_grad):
    f32 = jnp.float32
    bf16 = jnp.bfloat16
    tokens = latent.shape[1]
    width = PLAIN_HEAD_WIDTH + ROPE
    head_cols = ATTENTION_HEADS * PLAIN_HEAD_WIDTH
    lat = latent[0].astype(f32)
    inv_rms = lax.rsqrt(jnp.mean(lat * lat, axis=-1, keepdims=True) + eps)
    normed = lat * inv_rms
    nlat = (normed * latent_norm_gain).astype(bf16)
    stacked = jnp.stack([key_up_matrix, value_up_matrix])
    whole = lax.all_gather(stacked, "dp", axis=1, tiled=True)
    kv_tok = jnp.einsum("tc,gnc->tgn", nlat, whole, preferred_element_type=f32).astype(bf16)
    heads_query = query[0].reshape(tokens, ATTENTION_HEADS, width)
    key_nope = kv_tok[:, 0].reshape(tokens, ATTENTION_HEADS, PLAIN_HEAD_WIDTH)
    values = kv_tok[:, 1].reshape(tokens, ATTENTION_HEADS, VALUE_HEAD_WIDTH)
    d_out = out_grad[0].reshape(tokens, ATTENTION_HEADS, VALUE_HEAD_WIDTH)
    packed = jnp.concatenate([heads_query, key_nope, values, d_out], axis=2)
    arrived = lax.all_to_all(packed, "sp", split_axis=1, concat_axis=0, tiled=True)
    rope_full = lax.all_gather(rope_key[0], "sp", axis=0, tiled=True)
    grads_heads, rope_full_grad = attend_backward(arrived, rope_full)
    returned = lax.all_to_all(grads_heads, "sp", split_axis=0, concat_axis=1, tiled=True)
    rope_grad = lax.psum_scatter(rope_full_grad, "sp", scatter_dimension=0, tiled=True)
    query_grad = returned[:, :, :width].reshape(tokens, ATTENTION_HEADS * width)
    key_cols = returned[:, :, width : width + PLAIN_HEAD_WIDTH].reshape(tokens, head_cols)
    value_cols = returned[:, :, width + PLAIN_HEAD_WIDTH :].reshape(tokens, head_cols)
    dkv = jnp.stack([key_cols, value_cols], axis=1)
    d_nlat = jnp.einsum("tgn,gnc->tc", dkv, whole, preferred_element_type=f32)
    latents_all = lax.all_gather(nlat[None], "dp", axis=0, tiled=True)
    columns = lax.all_to_all(dkv[None], "dp", split_axis=3, concat_axis=0, tiled=True)
    partial_value = jnp.einsum("stgr,stc->grc", columns, latents_all, preferred_element_type=f32)
    weight_grads = lax.psum(partial_value, "sp")
    gain_grad = lax.psum(jnp.sum(d_nlat * normed, axis=0), ("sp", "dp"))
    scaled = d_nlat * latent_norm_gain
    latent_grad = inv_rms * (scaled - normed * jnp.mean(scaled * normed, axis=-1, keepdims=True))
    return (
        query_grad[None],
        latent_grad[None],
        rope_grad[None],
        weight_grads[0],
        weight_grads[1],
        gain_grad,
    )


def solution(mesh):
    in_specs = (
        P("dp", "sp", None),
        P("dp", "sp", None),
        P("dp", "sp", None),
        P(),
        P("dp", None),
        P("dp", None),
        P("dp", "sp", None),
    )
    out_specs = (
        P("dp", "sp", None),
        P("dp", "sp", None),
        P("dp", "sp", None),
        P("dp", None),
        P("dp", None),
        P(),
    )
    return jax.shard_map(local, mesh=mesh, in_specs=in_specs, out_specs=out_specs, check_vma=False)
```

profile of v0, /device:TPU:0, one launch (start us, length us, event | category | flops | bytes accessed | tf_op | source)
XLA Modules:
  0.0 738.0 jit_solution(6265751976223707838)
XLA Ops:
  7.2 3.1 pad_maximum_fusion.2
  12.3 3.9 reshape_squeeze.12
  16.4 55.1 %all-gather.4.cloned.1.call-done = bf16[2,2048,1024]{2,1,0:T(8,128)(2,1)} async-done(((bf16[2,512,1024]{2,1,0:T(8,128)(2,1)}), bf16[2,2048,1024]{2,1,0:T(8,128)(2,1)}) %all-gather.4.cloned.1.call-update) | async-done | bytes 8388624 | tf_op jit(solution)/shard_map/all_gather | solution.py:99
  71.5 6.2 convolution_convert_fusion
  84.6 3.1 copy.95
  87.8 5.6 pad_maximum_fusion
  93.4 4.0 copy.97
  97.4 5.6 all-to-all-start
  103.2 126.8 %all-gather = bf16[1,1536,32]{2,0,1:T(2,128)(2,1)S(1)} all-gather(bf16[1,192,32]{2,0,1:T(2,128)(2,1)S(1)} %copy.99), channel_id=2, replica_groups=mesh['sp'=8,'dp'=4] {'sp'}, dimensions={1}, use_global_device_ids=true | all-gather | bytes 110592 | tf_op jit(solution)/shard_map/all_gather | solution.py:107
  236.4 8.3 %copy.98 = bf16[8,192,4,288]{1,0,3,2:T(8,128)(2,1)} copy(bf16[8,192,4,288]{3,1,2,0:T(8,128)(2,1)} %bitcast.8) | data formatting | bytes 7077888 | tf_op jit(solution)/shard_map/all_to_all | solution.py:106
  244.7 6.9 all_to_all.42
  254.7 3.3 fusion.152
  258.0 5.4 fusion.43
  263.4 3.1 multiply_reduce_fusion.2
  274.4 3.2 fusion.6
  280.8 2.8 multiply_reduce_fusion.1
  283.7 9.7 %multiply_convert_fusion.1 = bf16[4,512,1024]{2,1,0:T(8,128)(2,1)S(1)} fusion(f32[4,512,1024]{2,1,0:T(8,128)S(1)} %get-tuple-element.177, f32[4,512]{1,0:T(4,128)S(1)} %get-tuple-element.176, f32[4,512,1024]{2,1,0:T(8,128)S(1)} %get-tuple-element.171, f32[4,512]{1,0:T(4,128)S(1)} %get-tuple-element.170), kind=kLoop, calls=%fused_computation.12 | loop fusion | flops 8388608 | bytes 20987904 | tf_op jit(solution)/shard_map/convert_element_type | solution.py:68
  295.5 3.1 fusion.50
  300.5 8.5 %fusion.4 = f32[4,512,1536]{2,1,0:T(8,128)} fusion(f32[1536,512,4]{0,1,2:T(8,128)S(1)} %fusion.114, pred[512,1536]{1,0:T(8,128)(4,1)S(1)} %copy-done.13, bf16[1536,4,288]{0,2,1:T(8,128)(2,1)} %copy-done.3), kind=kOutput, calls=%fused_computation.5 | convolution fusion | flops 412090368 | bytes 27000832 | tf_op jit(solution)/shard_map/qhd,khd->hqk/dot_general | solution.py:57
  309.1 14.9 %fusion.154 = (f32[4,512]{1,0:T(4,128)S(1)}, f32[4,512,1536]{2,1,0:T(8,128)}) fusion(f32[4,512,1536]{2,1,0:T(8,128)} %fusion.4), kind=kOutput, calls=%fused_computation.226 | output fusion | flops 6292991 | bytes 25174016 | tf_op jit(solution)/shard_map/sub | solution.py:65
  323.9 11.8 %multiply_reduce_fusion = (f32[4,512]{1,0:T(4,128)S(1)}, f32[4,512,1536]{2,1,0:T(8,128)}) fusion(f32[4,512,1536]{2,1,0:T(8,128)} %get-tuple-element.173, f32[4,512]{1,0:T(4,128)S(1)} %get-tuple-element.172, bf16[1536,4,288]{0,2,1:T(8,128)(2,1)} %copy-done.3), kind=kOutput, calls=%fused_computation.7 | convolution fusion | flops 412088320 | bytes 26230784 | tf_op jit(solution)/shard_map/qhd,khd->hqk/dot_general | solution.py:66
  335.7 6.0 multiply_convert_fusion
  341.8 4.5 fusion.52
  346.3 2.7 fusion.53
  351.6 11.2 %fusion.37 = f32[1536,4,64]{0,2,1:T(8,128)} fusion(f32[1536,4,64]{0,2,1:T(8,128)} %scatter-add.24, bf16[1536,4,288]{0,2,1:T(8,128)(2,1)} %copy-done.3, f32[4,512]{1,0:T(4,128)S(1)} %get-tuple-element.170, f32[4,512,1024]{2,1,0:T(8,128)} %copy-done.2), kind=kOutput, calls=%fused_computation.53 | convolution fusion | flops 274992128 | bytes 19144704 | tf_op jit(solution)/shard_map/hqk,qhd->khd/dot_general | solution.py:81
  362.8 4.4 fusion.42
  367.2 13.7 %fusion.22 = bf16[1536,4,64]{0,2,1:T(8,128)(2,1)} fusion(f32[1536,4,64]{0,2,1:T(8,128)} %fusion.37, bf16[1536,4,288]{0,2,1:T(8,128)(2,1)} %copy-done.3, f32[4,512]{1,0:T(4,128)S(1)} %get-tuple-element.172, f32[4,512,1536]{2,1,0:T(8,128)} %fusion.4), kind=kOutput, calls=%fused_computation.36 | convolution fusion | flops 412880384 | bytes 27795456 | tf_op jit(solution)/shard_map/hqk,qhd->khd/dot_general | solution.py:81
  381.0 4.6 fusion.21
  385.9 3.0 pad_maximum_fusion.1
  388.8 5.8 copy.107
  394.6 4.6 all-to-all-start.1
  401.9 64.4 %all-to-all-done.1 = bf16[1536,4,224]{2,1,0:T(4,128)(2,1)} async-done(((bf16[1536,4,224]{2,1,0:T(4,128)(2,1)}), bf16[1536,4,224]{2,1,0:T(4,128)(2,1)}, u32[]{:S(2)}, u32[]{:S(2)}) %all-to-all-start.1) | async-done | bytes 2752544 | tf_op jit(solution)/shard_map/all_to_all | solution.py:109
  468.8 2.8 fusion.149
  471.5 2.6 copy.111
  481.1 2.7 fusion.60
  483.8 6.1 copy.116
  489.8 4.4 all-to-all-start.2
  494.3 3.7 fusion.58
  498.0 4.0 fusion.26
  503.7 16.3 %all-to-all-done.2 = bf16[1,192,2,2048]{1,2,0,3:T(2,128)(2,1)} async-done(((bf16[1,192,2,2048]{1,2,0,3:T(2,128)(2,1)}), bf16[1,192,2,2048]{1,2,0,3:T(2,128)(2,1)}, u32[]{:S(2)}, u32[]{:S(2)}) %all-to-all-start.2) | async-done | bytes 1572896 | tf_op jit(solution)/shard_map/all_to_all | solution.py:117
  520.0 6.0 copy.118
  526.0 5.7 convolution_bitcast_fusion.1
  531.7 34.6 %reduce-scatter.4.cloned.1.call-done = f32[192,32]{1,0:T(8,128)} async-done(((f32[1536,32]{1,0:T(8,128)}), f32[192,32]{1,0:T(8,128)}) %reduce-scatter.4.cloned.1.call-update) | async-done | bytes 24592
  569.2 3.0 broadcast_in_dim_reshape.3
  572.2 6.3 fusion.72
  578.5 44.0 %psum.15 = f32[1024]{0:T(1024)} all-reduce(f32[1024]{0:T(1024)S(1)} %get-tuple-element.138), channel_id=1, replica_groups=mesh['sp'=8,'dp'=4] {'sp','dp'}, use_global_device_ids=true, to_apply=%region_14.15 | all-reduce | flops 1024 | bytes 8192 | tf_op jit(solution)/shard_map/psum | solution.py:120
  623.6 102.6 %all-reduce.5.cloned.1.call-done = f32[2,512,1024]{2,1,0:T(8,128)} async-done(((f32[2,512,1024]{2,1,0:T(8,128)}), f32[2,512,1024]{2,1,0:T(8,128)}) %all-reduce.5.cloned.1.call-update) | async-done | bytes 4194320 | tf_op jit(solution)/shard_map/psum | solution.py:119
  726.2 4.8 slice_bitcast_fusion
  (168 shorter events, 54.3 us)
Async XLA Ops:
  7.2 3.2 copy-start.32
  7.2 64.3 %all-gather.4.cloned.1.call-start = ((), (), s32[]{:S(2)}) async-start(), calls=%async_computation.4 | async-start | bytes 10485760 | tf_op jit(solution)/shard_map/all_gather | solution.py:99
  10.3 5.9 copy-start.10
  10.4 61.1 %copy-start.41 = (f32[1024]{0:T(1024)S(1)}, f32[1024]{0:T(1024)}, u32[]{:S(2)}) copy-start(f32[1024]{0:T(1024)} %param.34) | copy-start | bytes 12292
  16.4 55.1 %copy-start.44 = (f32[192]{0:T(256)}, f32[192]{0:T(256)S(1)}, u32[]{:S(2)}) copy-start(f32[192]{0:T(256)S(1)} %add_rsqrt_fusion) | copy-start | bytes 2308
  97.4 5.7 copy-start.43
  97.4 139.0 %all-to-all-start = ((bf16[192,32,288]{2,0,1:T(8,128)(2,1)}), bf16[192,32,288]{2,0,1:T(8,128)(2,1)}, u32[]{:S(2)}, u32[]{:S(2)}) async-start(bf16[192,32,288]{2,0,1:T(8,128)(2,1)} %copy.97), calls=%async_computation | async-start | bytes 9437184 | tf_op jit(solution)/shard_map/all_to_all | solution.py:106
  251.6 11.8 %copy-start.3 = (bf16[1536,4,288]{0,2,1:T(8,128)(2,1)}, bf16[1536,4,288]{0,2,1:T(8,128)(2,1)S(1)}, u32[]{:S(2)}) copy-start(bf16[1536,4,288]{0,2,1:T(8,128)(2,1)S(1)} %all_to_all.42) | copy-start | bytes 10616836
  251.6 2.0 copy-start.16
  251.6 2.0 copy-start.18
  251.6 2.0 copy-start.24
  254.7 3.3 copy-start.5
  263.4 3.4 copy-start.4
  268.0 5.0 copy-start.7
  268.0 5.0 copy-start.9
  277.6 3.3 copy-start.2
  293.4 5.2 copy-start.1
  298.7 1.8 copy-start.13
  323.9 11.8 %slice-start = ((s8[12582912]{0:T(1024)(128)(4,1)}), s8[4194304]{0:T(1024)(128)(4,1)S(1)}, s32[]{:S(2)}) async-start(s8[12582912]{0:T(1024)(128)(4,1)} %bitcast.187), calls=%async_computation.8 | async-start | bytes 8388608
  323.9 11.8 %slice-start.1 = ((s8[12582912]{0:T(1024)(128)(4,1)}), s8[4194304]{0:T(1024)(128)(4,1)S(1)}, s32[]{:S(2)}) async-start(s8[12582912]{0:T(1024)(128)(4,1)} %bitcast.187), calls=%async_computation.9 | async-start | bytes 8388608
  323.9 11.8 %slice-start.2 = ((s8[12582912]{0:T(1024)(128)(4,1)}), s8[4194304]{0:T(1024)(128)(4,1)S(1)}, s32[]{:S(2)}) async-start(s8[12582912]{0:T(1024)(128)(4,1)} %bitcast.187), calls=%async_computation.10 | async-start | bytes 8388608
  341.8 7.1 copy-start
  346.3 2.7 copy-start.34
  380.9 4.7 copy-start.21
  380.9 4.8 copy-start.39
  380.9 4.8 copy-start.40
  380.9 4.8 copy-start.22
  380.9 4.8 copy-start.37
  380.9 4.8 copy-start.38
  380.9 4.9 copy-start.23
  380.9 4.9 copy-start.35
  380.9 4.9 copy-start.36
  380.9 4.9 copy-start.25
  381.0 4.9 copy-start.26
  381.0 4.9 copy-start.27
  381.0 4.9 copy-start.33
  394.6 4.9 copy-start.11
  394.6 4.9 copy-start.42
  394.6 4.9 copy-start.45
  394.6 71.6 %all-to-all-start.1 = ((bf16[1536,4,224]{2,1,0:T(4,128)(2,1)}), bf16[1536,4,224]{2,1,0:T(4,128)(2,1)}, u32[]{:S(2)}, u32[]{:S(2)}) async-start(bf16[1536,4,224]{2,1,0:T(4,128)(2,1)} %copy.107), calls=%async_computation.1 | async-start | bytes 6291456 | tf_op jit(solution)/shard_map/all_to_all | solution.py:109
  399.2 126.8 %all-gather.6.cloned.1.call-start = ((), (), s32[]{:S(2)}) async-start(), calls=%async_computation.5 | async-start | bytes 1966080 | tf_op jit(solution)/shard_map/all_gather | solution.py:116
  489.8 30.2 %all-to-all-start.2 = ((bf16[1,192,2,2048]{1,2,0,3:T(2,128)(2,1)}), bf16[1,192,2,2048]{1,2,0,3:T(2,128)(2,1)}, u32[]{:S(2)}, u32[]{:S(2)}) async-start(bf16[1,192,2,2048]{1,2,0,3:T(2,128)(2,1)} %copy.116), calls=%async_computation.2 | async-start | bytes 4194304 | tf_op jit(solution)/shard_map/all_to_all | solution.py:117
  494.3 72.0 %reduce-scatter.4.cloned.1.call-start = ((), (), s32[]{:S(2)}) async-start(), calls=%async_computation.7 | async-start | bytes 884736
  498.0 4.0 copy-start.47
  503.6 222.6 %all-reduce.5.cloned.1.call-start = ((), (), s32[]{:S(2)}) async-start(), calls=%async_computation.6 | async-start | bytes 8388608 | tf_op jit(solution)/shard_map/psum | solution.py:119
  567.9 4.3 copy-start.12
  568.2 4.0 copy-start.14
  568.2 4.0 copy-start.15
  (10 other events, 9.7 us)
Sparse Core Ops, SparseCore 0:
  10.5 60.9 all-gather.3
  401.6 19.9 all-gather.5
  503.8 62.4 reduce-scatter.3
  569.8 156.3 all-reduce.4
where the time goes:
time: 747 us; the launch traced here: 738 us
  waiting for transfers between devices  273 us (37%)
  blocking collectives  171 us (23%)
  matrix products  118 us (16%)
  local copies, waits for them, and re-layouts  87 us (12%)
  other arithmetic  59.6 us (8%)
  starting transfers between devices  15.1 us (2%)
  between operations  15 us (2%)
    all_gather x1, blocking collectives, local(): rope_full = lax.all_gather(rope_key[0], 'sp', axis=0, tiled=True)  127 us
    psum x1, waiting for transfers between devices, local(): weight_grads = lax.psum(partial_value, 'sp')  103 us
    all_to_all x1, waiting for transfers between devices, local(): lax.all_to_all(grads_heads, 'sp', split_axis=0, concat_axis=1, tiled=True)  64.4 us
    all_gather x1, waiting for transfers between devices, local(): whole = lax.all_gather(stacked, 'dp', axis=1, tiled=True)  55.1 us
    psum x1, blocking collectives, local(): gain_grad = lax.psum(jnp.sum(d_nlat * normed, axis=0), ('sp', 'dp'))  44 us
    unnamed x5, waiting for transfers between devices  34.6 us
    dot_general x3, matrix products, attend_backward(): jnp.einsum('hqk,qhd->khd', p_b, go, preferred_element_type=f32)  30.3 us
    sub x3, other arithmetic, attend_backward(): probs = jax.nn.softmax(scores, axis=-1)  20.1 us
  transfers between devices with their start and end apart: 7, of which 5 were waited for; matrix products, arithmetic and copies ran while one was open for 10% of the time, Pallas kernels for 0%

commit v1 on v0

--- a/solution.py
+++ b/solution.py
@@ -116,7 +116,8 @@
     latents_all = lax.all_gather(nlat[None], "dp", axis=0, tiled=True)
     columns = lax.all_to_all(dkv[None], "dp", split_axis=3, concat_axis=0, tiled=True)
     partial_value = jnp.einsum("stgr,stc->grc", columns, latents_all, preferred_element_type=f32)
-    weight_grads = lax.psum(partial_value, "sp")
+    parts = lax.all_gather(partial_value, "sp")
+    weight_grads = jnp.sum(parts, axis=0)
     gain_grad = lax.psum(jnp.sum(d_nlat * normed, axis=0), ("sp", "dp"))
     scaled = d_nlat * latent_norm_gain
     latent_grad = inv_rms * (scaled - normed * jnp.mean(scaled * normed, axis=-1, keepdims=True))

time: 747 us -> 1240 us (1.66)
  waiting for transfers between devices: 273 us -> 716 us
  blocking collectives: 171 us -> 208 us
  other arithmetic: 59.6 us -> 74.4 us
    all_gather x0 -> x1, waiting for transfers between devices: none -> 546 us  [local(): parts = lax.all_gather(partial_value, 'sp')]
    psum x1 -> x0, waiting for transfers between devices: 103 us -> none  [local(): weight_grads = lax.psum(partial_value, 'sp')]
    psum x1, blocking collectives: 44 us -> 80.7 us  [local(): gain_grad = lax.psum(jnp.sum(d_nlat * normed, axis=0), ('sp', 'dp'))]
    reduce_sum x0 -> x1, other arithmetic: none -> 14.7 us  [local(): weight_grads = jnp.sum(parts, axis=0)]
  transfers between devices with their start and end apart: 7 -> 7, of which waited for: 5 -> 5; matrix products, arithmetic and copies ran while one was open for 10% -> 6% of each run, Pallas kernels for 0% -> 0%
where the time goes in v1:
time: 1240 us; the launch traced here: 1230 us
  waiting for transfers between devices  716 us (58%)
  blocking collectives  208 us (17%)
  matrix products  117 us (9%)
  local copies, waits for them, and re-layouts  86.9 us (7%)
  other arithmetic  74.4 us (6%)
  starting transfers between devices  15.1 us (1%)
  between operations  15 us (1%)
    all_gather x1, waiting for transfers between devices, local(): parts = lax.all_gather(partial_value, 'sp')  546 us
    all_gather x1, blocking collectives, local(): rope_full = lax.all_gather(rope_key[0], 'sp', axis=0, tiled=True)  127 us
    psum x1, blocking collectives, local(): gain_grad = lax.psum(jnp.sum(d_nlat * normed, axis=0), ('sp', 'dp'))  80.7 us
    all_to_all x1, waiting for transfers between devices, local(): lax.all_to_all(grads_heads, 'sp', split_axis=0, concat_axis=1, tiled=True)  64.4 us
    all_gather x1, waiting for transfers between devices, local(): whole = lax.all_gather(stacked, 'dp', axis=1, tiled=True)  55.1 us
    unnamed x5, waiting for transfers between devices  34.5 us
    dot_general x3, matrix products, attend_backward(): jnp.einsum('hqk,qhd->khd', p_b, go, preferred_element_type=f32)  30.2 us
  transfers between devices with their start and end apart: 7, of which 5 were waited for; matrix products, arithmetic and copies ran while one was open for 6% of the time, Pallas kernels for 0%

profile of v1, /device:TPU:0, one launch (start us, length us, event | category | flops | bytes accessed | tf_op | source)
XLA Modules:
  0.0 1232.3 jit_solution(11881398365884502534)
XLA Ops:
  7.2 3.1 pad_maximum_fusion.2
  12.3 3.9 reshape_squeeze.12
  16.4 55.1 %all-gather.6.cloned.1.call-done = bf16[2,2048,1024]{2,1,0:T(8,128)(2,1)} async-done(((bf16[2,512,1024]{2,1,0:T(8,128)(2,1)}), bf16[2,2048,1024]{2,1,0:T(8,128)(2,1)}) %all-gather.6.cloned.1.call-update) | async-done | bytes 8388624 | tf_op jit(solution)/shard_map/all_gather | solution.py:99
  71.5 6.2 convolution_convert_fusion
  84.6 3.1 copy.95
  87.8 5.6 pad_maximum_fusion
  93.4 4.0 copy.97
  97.4 5.6 all-to-all-start
  103.2 126.8 %all-gather = bf16[1,1536,32]{2,0,1:T(2,128)(2,1)S(1)} all-gather(bf16[1,192,32]{2,0,1:T(2,128)(2,1)S(1)} %copy.99), channel_id=2, replica_groups=mesh['sp'=8,'dp'=4] {'sp'}, dimensions={1}, use_global_device_ids=true | all-gather | bytes 110592 | tf_op jit(solution)/shard_map/all_gather | solution.py:107
  236.4 8.3 copy.98
  244.7 6.9 all_to_all.42
  254.7 3.3 fusion.152
  258.0 5.4 fusion.43
  263.3 3.1 multiply_reduce_fusion.2
  274.3 3.2 fusion.6
  280.8 2.8 multiply_reduce_fusion.1
  283.6 9.7 multiply_convert_fusion.1
  295.5 3.1 fusion.50
  300.5 8.5 fusion.4
  309.0 14.9 %fusion.154 = (f32[4,512]{1,0:T(4,128)S(1)}, f32[4,512,1536]{2,1,0:T(8,128)}) fusion(f32[4,512,1536]{2,1,0:T(8,128)} %fusion.4), kind=kOutput, calls=%fused_computation.226 | output fusion | flops 6292991 | bytes 25174016 | tf_op jit(solution)/shard_map/sub | solution.py:65
  323.9 11.8 multiply_reduce_fusion
  335.7 6.0 multiply_convert_fusion
  341.8 4.5 fusion.52
  346.2 2.7 fusion.53
  351.6 11.1 fusion.37
  362.7 4.4 fusion.42
  367.1 13.7 %fusion.22 = bf16[1536,4,64]{0,2,1:T(8,128)(2,1)} fusion(f32[1536,4,64]{0,2,1:T(8,128)} %fusion.37, bf16[1536,4,288]{0,2,1:T(8,128)(2,1)} %copy-done.3, f32[4,512]{1,0:T(4,128)S(1)} %get-tuple-element.172, f32[4,512,1536]{2,1,0:T(8,128)} %fusion.4), kind=kOutput, calls=%fused_computation.36 | convolution fusion | flops 412880384 | bytes 27795456 | tf_op jit(solution)/shard_map/hqk,qhd->khd/dot_general | solution.py:81
  380.9 4.6 fusion.21
  385.8 3.0 pad_maximum_fusion.1
  388.8 5.8 copy.107
  394.6 4.6 all-to-all-start.1
  401.8 64.4 %all-to-all-done.1 = bf16[1536,4,224]{2,1,0:T(4,128)(2,1)} async-done(((bf16[1536,4,224]{2,1,0:T(4,128)(2,1)}), bf16[1536,4,224]{2,1,0:T(4,128)(2,1)}, u32[]{:S(2)}, u32[]{:S(2)}) %all-to-all-start.1) | async-done | bytes 2752544 | tf_op jit(solution)/shard_map/all_to_all | solution.py:109
  468.7 2.8 fusion.149
  481.0 2.7 fusion.60
  483.7 6.1 copy.116
  489.8 4.4 all-to-all-start.2
  494.3 3.7 fusion.58
  497.9 4.0 fusion.26
  503.6 16.3 %all-to-all-done.2 = bf16[1,192,2,2048]{1,2,0,3:T(2,128)(2,1)} async-done(((bf16[1,192,2,2048]{1,2,0,3:T(2,128)(2,1)}), bf16[1,192,2,2048]{1,2,0,3:T(2,128)(2,1)}, u32[]{:S(2)}, u32[]{:S(2)}) %all-to-all-start.2) | async-done | bytes 1572896 | tf_op jit(solution)/shard_map/all_to_all | solution.py:117
  519.9 6.0 copy.118
  526.0 5.8 convolution_bitcast_fusion.1
  531.8 34.5 %reduce-scatter.4.cloned.1.call-done = f32[192,32]{1,0:T(8,128)} async-done(((f32[1536,32]{1,0:T(8,128)}), f32[192,32]{1,0:T(8,128)}) %reduce-scatter.4.cloned.1.call-update) | async-done | bytes 24592
  569.2 3.0 broadcast_in_dim_reshape.3
  572.1 6.1 fusion.72
  578.3 80.7 %psum.7 = f32[1024]{0:T(1024)} all-reduce(f32[1024]{0:T(1024)S(1)} %get-tuple-element.138), channel_id=1, replica_groups=mesh['sp'=8,'dp'=4] {'sp','dp'}, use_global_device_ids=true, to_apply=%region_14.15 | all-reduce | flops 1024 | bytes 8192 | tf_op jit(solution)/shard_map/psum | solution.py:121
  660.1 545.7 %all-gather.10.cloned.1.call-done = f32[16,512,1024]{2,1,0:T(8,128)} async-done(((f32[2,512,1024]{2,1,0:T(8,128)}), f32[16,512,1024]{2,1,0:T(8,128)}) %all-gather.10.cloned.1.call-update) | async-done | bytes 33554448 | tf_op jit(solution)/shard_map/all_gather | solution.py:119
  1205.7 14.7 %reduce_sum.98 = f32[2,512,1024]{2,1,0:T(8,128)} reduce(f32[8,2,512,1024]{3,2,1,0:T(8,128)} %bitcast.190, f32[]{:T(128)} %constant.315.clone.1), dimensions={0}, to_apply=%region_12.13 | reduce | flops 7340032 | bytes 37748740 | tf_op jit(solution)/shard_map/reduce_sum | solution.py:120
  1220.5 4.8 slice_bitcast_fusion
  (169 shorter events, 56.9 us)
Async XLA Ops:
  7.2 3.2 copy-start.32
  7.2 64.3 %all-gather.6.cloned.1.call-start = ((), (), s32[]{:S(2)}) async-start(), calls=%async_computation.4 | async-start | bytes 10485760 | tf_op jit(solution)/shard_map/all_gather | solution.py:99
  10.3 5.9 copy-start.10
  10.4 61.1 %copy-start.41 = (f32[1024]{0:T(1024)S(1)}, f32[1024]{0:T(1024)}, u32[]{:S(2)}) copy-start(f32[1024]{0:T(1024)} %param.34) | copy-start | bytes 12292
  16.4 55.1 %copy-start.44 = (f32[192]{0:T(256)}, f32[192]{0:T(256)S(1)}, u32[]{:S(2)}) copy-start(f32[192]{0:T(256)S(1)} %add_rsqrt_fusion) | copy-start | bytes 2308
  97.4 5.7 copy-start.43
  97.4 139.0 %all-to-all-start = ((bf16[192,32,288]{2,0,1:T(8,128)(2,1)}), bf16[192,32,288]{2,0,1:T(8,128)(2,1)}, u32[]{:S(2)}, u32[]{:S(2)}) async-start(bf16[192,32,288]{2,0,1:T(8,128)(2,1)} %copy.97), calls=%async_computation | async-start | bytes 9437184 | tf_op jit(solution)/shard_map/all_to_all | solution.py:106
  251.6 11.8 copy-start.3
  251.6 2.0 copy-start.16
  251.6 2.0 copy-start.18
  251.6 2.0 copy-start.24
  254.7 3.3 copy-start.5
  263.3 3.4 copy-start.4
  268.0 5.0 copy-start.7
  268.0 5.0 copy-start.9
  277.5 3.3 copy-start.2
  293.4 5.2 copy-start.1
  298.6 1.8 copy-start.13
  323.9 11.8 slice-start
  323.9 11.8 slice-start.1
  323.9 11.8 slice-start.2
  341.8 7.1 copy-start
  346.2 2.7 copy-start.34
  380.8 4.7 copy-start.21
  380.8 4.8 copy-start.39
  380.8 4.8 copy-start.40
  380.8 4.8 copy-start.22
  380.8 4.8 copy-start.37
  380.8 4.8 copy-start.38
  380.8 4.9 copy-start.23
  380.9 4.9 copy-start.35
  380.9 4.9 copy-start.36
  380.9 4.9 copy-start.25
  380.9 4.9 copy-start.26
  380.9 4.9 copy-start.27
  380.9 4.9 copy-start.33
  394.5 4.9 copy-start.11
  394.5 4.9 copy-start.42
  394.5 4.9 copy-start.45
  394.6 71.6 %all-to-all-start.1 = ((bf16[1536,4,224]{2,1,0:T(4,128)(2,1)}), bf16[1536,4,224]{2,1,0:T(4,128)(2,1)}, u32[]{:S(2)}, u32[]{:S(2)}) async-start(bf16[1536,4,224]{2,1,0:T(4,128)(2,1)} %copy.107), calls=%async_computation.1 | async-start | bytes 6291456 | tf_op jit(solution)/shard_map/all_to_all | solution.py:109
  399.1 126.8 %all-gather.8.cloned.1.call-start = ((), (), s32[]{:S(2)}) async-start(), calls=%async_computation.5 | async-start | bytes 1966080 | tf_op jit(solution)/shard_map/all_gather | solution.py:116
  489.8 30.2 %all-to-all-start.2 = ((bf16[1,192,2,2048]{1,2,0,3:T(2,128)(2,1)}), bf16[1,192,2,2048]{1,2,0,3:T(2,128)(2,1)}, u32[]{:S(2)}, u32[]{:S(2)}) async-start(bf16[1,192,2,2048]{1,2,0,3:T(2,128)(2,1)} %copy.116), calls=%async_computation.2 | async-start | bytes 4194304 | tf_op jit(solution)/shard_map/all_to_all | solution.py:117
  494.2 72.0 %reduce-scatter.4.cloned.1.call-start = ((), (), s32[]{:S(2)}) async-start(), calls=%async_computation.7 | async-start | bytes 884736
  497.9 4.0 copy-start.47
  503.6 702.2 %all-gather.10.cloned.1.call-start = ((), (), s32[]{:S(2)}) async-start(), calls=%async_computation.6 | async-start | bytes 37748736 | tf_op jit(solution)/shard_map/all_gather | solution.py:119
  567.8 4.3 copy-start.12
  568.1 4.0 copy-start.14
  568.1 4.0 copy-start.15
  (10 other events, 9.7 us)
Sparse Core Ops, SparseCore 0:
  10.5 60.9 all-gather.5
  401.5 19.9 all-gather.7
  503.7 62.4 reduce-scatter.3
  567.6 638.0 all-gather.9
